TPU v7x, 128 devices: a whole 4x4x4 slice. The times are simulated.
128 devices in a mesh: ra: 16 (over z, y), cb: 4 (over x), dp: 2 (over core).
Axes of the slice: x: 4, y: 4, z: 4, core: 2. Of those that a mesh axis runs over, the one named last changes fastest.
Arguments:
- tokens: bfloat16 [3072, 4096], P('dp', 'ra'), may hold values from -20 to 20
- pre_gain: float32 [4096], P('ra'), may hold values from 0.1 to 1.9
- up_weight: bfloat16 [4096, 16384], P('ra', 'cb'), may hold values from -0.09375 to 0.09375
- up_bias: float32 [16384], P('cb'), may hold values from -4 to 4
- down_weight: bfloat16 [16384, 4096], P('cb', 'ra'), may hold values from -0.046875 to 0.046875
- post_gain: float32 [4096], P('ra'), may hold values from 0.1 to 1.9
Outputs:
- stream_out: bfloat16 [3072, 4096], P('dp', 'ra')
All inputs are finite; a program needn't handle non-finite values.
Results may differ from a plain program's by a relative error of at most 0.0051.
Values may be sent and summed in bfloat16 or wider, within the bound.
A program may use at most 128 MiB of HBM per device.

v0:
```python
import jax
import jax.numpy as jnp
from jax import lax
from jax.sharding import PartitionSpec as P

D = 4096


epsilon = 1e-06
residual_weight = 0.5


def in_blocks(array, dim, size):
    before, after = (array.shape[:dim], array.shape[dim + 1 :])
    return jnp.moveaxis(array.reshape(*before, size, -1, *after), dim, 0)


def sent_and_summed(array, axis, dim):
    size = lax.axis_size(axis)
    pieces = lax.all_to_all(in_blocks(array, dim, size), axis, 0, 0, tiled=True)
    return jnp.sum(pieces, axis=0)


def from_everyone(array, axis):
    copies = jnp.broadcast_to(array, (lax.axis_size(axis), *array.shape))
    return lax.all_to_all(copies, axis, split_axis=0, concat_axis=0, tiled=True)


def of_everyone(array, axis):
    return from_everyone(array, axis).sum(axis=0)


def activate(summed, inverse, offset):
    return jnp.square(jax.nn.relu(summed * inverse[:, None] + offset)).astype(jnp.bfloat16)


def body(tokens, pre_gain, up_weight, up_bias, down_weight, post_gain):
    stream = tokens.astype(jnp.float32)
    energy = jnp.sum(stream * stream, axis=1)
    scaled = (stream * pre_gain).astype(jnp.bfloat16)
    partial_value = jnp.dot(scaled, up_weight, preferred_element_type=jnp.float32)
    total = sent_and_summed(energy, "ra", 0)
    share = lax.psum_scatter(partial_value, "ra", scatter_dimension=0, tiled=True)
    hidden = activate(share, lax.rsqrt(total / D + epsilon), up_bias)
    branch = jnp.dot(
        lax.all_gather(hidden, "ra", axis=0, tiled=True),
        down_weight,
        preferred_element_type=jnp.float32,
    )
    branch = lax.psum(branch, "cb")
    branch_energy = of_everyone(jnp.sum(branch * branch, axis=1), "ra")
    normed = branch * lax.rsqrt(branch_energy / D + epsilon)[:, None] * post_gain
    return (residual_weight * stream + normed).astype(jnp.bfloat16)


def solution(mesh):
    in_specs = (P("dp", "ra"), P("ra"), P("ra", "cb"), P("cb"), P("cb", "ra"), P("ra"))
    out_specs = P("dp", "ra")
    return jax.shard_map(body, mesh=mesh, in_specs=in_specs, out_specs=out_specs, check_vma=False)
```

profile of v0, /device:TPU:0, one launch (start us, length us, event | category | flops | bytes accessed | tf_op | source)
XLA Modules:
  0.0 353.1 jit_solution(17508895634542770596)
XLA Ops:
  6.5 0.0 copy-start
  6.5 0.0 reduce-scatter.2.cloned.1.call-start
  6.5 1.6 copy-done
  8.1 11.2 %fusion.4 = f32[1536,4096]{1,0:T(8,128)} fusion(bf16[256,4096]{1,0:T(8,128)(2,1)S(1)} %copy-done, bf16[1536,256]{1,0:T(8,128)(2,1)} %param.6, f32[256]{0:T(256)} %param.7), kind=kOutput, calls=%fused_computation.9 | convolution fusion | flops 3222405120 | bytes 28050432 | tf_op jit(solution)/shard_map/dot_general | solution.py:41
  19.4 0.0 reduce-scatter.2.cloned.1.call-update
  19.4 0.0 all-gather.2.cloned.1.call-start
  19.4 1.1 copy-done.1
  20.5 0.3 fusion.3
  20.8 0.1 all_to_all.10
  20.9 15.5 %all_to_all.15 = f32[16,1,96]{2,1,0:T(1,128)S(1)} all-to-all(f32[16,1,96]{2,1,0:T(1,128)S(1)} %all_to_all.10), channel_id=1, replica_groups=mesh['ra'=16,'cb'=4,'dp'=2] {'ra'}, dimensions={0} | all-to-all | bytes 12288 | tf_op jit(solution)/shard_map/all_to_all | solution.py:20
  36.4 138.9 %reduce-scatter.2.cloned.1.call-done = f32[96,4096]{1,0:T(8,128)} async-done(((f32[1536,4096]{1,0:T(8,128)}), f32[96,4096]{1,0:T(8,128)}) %reduce-scatter.2.cloned.1.call-update) | async-done | bytes 1572880 | tf_op jit(solution)/shard_map/reduce_scatter | solution.py:43
  175.3 0.0 copy-done.2
  175.3 2.6 multiply_convert_fusion
  177.9 0.0 all-gather.2.cloned.1.call-update
  178.0 0.0 all-reduce.2.cloned.1.call-start
  178.0 89.6 %all-gather.2.cloned.1.call-done = bf16[1536,4096]{1,0:T(8,128)(2,1)} async-done(((bf16[96,4096]{1,0:T(8,128)(2,1)}), bf16[1536,4096]{1,0:T(8,128)(2,1)}) %all-gather.2.cloned.1.call-update) | async-done | bytes 12582928 | tf_op jit(solution)/shard_map/all_gather | solution.py:46
  267.6 9.8 %fusion.7 = f32[1536,256]{1,0:T(8,128)} fusion(bf16[1536,4096]{1,0:T(8,128)(2,1)} %all-gather.2.cloned.1.call-done, bf16[4096,256]{1,0:T(8,128)(2,1)} %param.10), kind=kOutput, calls=%fused_computation.13 | convolution fusion | flops 3221225472 | bytes 16252928 | tf_op jit(solution)/shard_map/dot_general | solution.py:45
  277.4 0.0 all-reduce.2.cloned.1.call-update
  277.4 50.1 %all-reduce.2.cloned.1.call-done = f32[1536,256]{1,0:T(8,128)} async-done(((f32[1536,256]{1,0:T(8,128)}), f32[1536,256]{1,0:T(8,128)}) %all-reduce.2.cloned.1.call-update) | async-done | bytes 1572880 | tf_op jit(solution)/shard_map/psum | solution.py:50
  327.5 1.7 multiply_reduce_fusion
  329.2 0.1 broadcast_in_dim.2
  329.3 14.6 %all_to_all.16 = f32[16,1,1536]{2,1,0:T(1,128)S(1)} all-to-all(f32[16,1,1536]{2,1,0:T(1,128)S(1)} %broadcast_in_dim.2), channel_id=1, replica_groups=mesh['ra'=16,'cb'=4,'dp'=2] {'ra'}, dimensions={0} | all-to-all | bytes 196608 | tf_op jit(solution)/shard_map/all_to_all | solution.py:26
  343.9 0.1 reduce_sum.39
  343.9 2.6 fusion.1
  (7 shorter events, 0.0 us)
Async XLA Ops:
  6.5 1.6 copy-start
  6.5 168.8 %reduce-scatter.2.cloned.1.call-start = ((), (), s32[]{:S(2)}) async-start(), calls=%async_computation.3 | async-start | bytes 26738688 | tf_op jit(solution)/shard_map/reduce_scatter | solution.py:43
  19.4 1.1 copy-start.1
  19.4 156.0 %copy-start.2 = (f32[4096]{0:T(1024)S(1)}, f32[4096]{0:T(1024)}, u32[]{:S(2)}) copy-start(f32[4096]{0:T(1024)} %param.9) | copy-start | bytes 49156
  19.4 248.2 %all-gather.2.cloned.1.call-start = ((), (), s32[]{:S(2)}) async-start(), calls=%async_computation.4 | async-start | bytes 13369344 | tf_op jit(solution)/shard_map/all_gather | solution.py:46
  178.0 149.6 %all-reduce.2.cloned.1.call-start = ((), (), s32[]{:S(2)}) async-start(), calls=%async_computation.5 | async-start | bytes 3145728 | tf_op jit(solution)/shard_map/psum | solution.py:50
  277.4 66.5 %copy-start.3 = (f32[256]{0:T(256)S(1)}, f32[256]{0:T(256)}, u32[]{:S(2)}) copy-start(f32[256]{0:T(256)} %param.11) | copy-start | bytes 3076
Sparse Core Ops, SparseCore 0:
  19.5 155.7 reduce-scatter.1
  178.1 89.4 all-gather.1
  277.6 49.8 all-reduce.1
where the time goes:
time: 353 us
  waiting for transfers between devices  279 us (79%)
  blocking collectives  30.1 us (9%)
  matrix products  21.1 us (6%)
  between operations  13.2 us (4%)
  other arithmetic  7.27 us (2%)
    reduce_scatter x1, waiting for transfers between devices, body(): lax.psum_scatter(partial_value, 'ra', scatter_dimension=0, tiled=True)  139 us
    all_gather x1, waiting for transfers between devices, body(): lax.all_gather(hidden, 'ra', axis=0, tiled=True)  89.6 us
    psum x1, waiting for transfers between devices, body(): branch = lax.psum(branch, 'cb')  50.1 us
    all_to_all x1, blocking collectives, sent_and_summed(): pieces = lax.all_to_all(in_blocks(array, dim, size), axis, 0, 0, tiled=True)  15.5 us
    all_to_all x1, blocking collectives, from_everyone(): return lax.all_to_all(copies, axis, split_axis=0, concat_axis=0, tiled=True)  14.6 us
    dot_general x1, matrix products, body(): jnp.dot(scaled, up_weight, preferred_element_type=jnp.float32)  11.2 us
    dot_general x1, matrix products, body(): jnp.dot(lax.all_gather(hidden, 'ra', axis=0, tiled=True), down_weight, pr...  9.83 us
  transfers between devices with their start and end apart: 3, of which 3 were waited for; matrix products, arithmetic and copies ran while one was open for 0% of the time, Pallas kernels for 0%

commit v1 on v0

v1 whole, which is shorter than its diff:
```python
import functools

import jax
import jax.numpy as jnp
from jax import lax
from jax.experimental import pallas as pl
from jax.experimental.pallas import tpu as pltpu
from jax.sharding import PartitionSpec as P

MESH = pl.DeviceIdType.MESH
D = 4096
CHUNKS = 6
epsilon = 1e-06
residual_weight = 0.5
f32, bf16 = jnp.float32, jnp.bfloat16


def lane_sums_as_row(square):
    ones = jnp.ones((8, square.shape[1]), bf16)
    high = square.astype(bf16)
    low = (square - high.astype(f32)).astype(bf16)
    contract = (((1,), (1,)), ((), ()))
    total = lax.dot_general(ones, high, contract, preferred_element_type=f32)
    return total + lax.dot_general(ones, low, contract, preferred_element_type=f32)


def kernel(
    tok, pre_gain, up_bias, post_gain, up_hbm, down_hbm, out,
    xg, wu, wd, ps, pr, hg, os, zr, xs, xr, br, inv_col,
    e_own, e_in, be, be_in,
    ssem, rsem, wssem, wrsem, lsem,
):
    C, _, Q, _ = tok.shape
    R = 4 * Q
    ra, x, k = lax.axis_index("ra"), lax.axis_index("cb"), lax.axis_index("dp")
    z, y = ra // 4, ra % 4

    def peer(axis, j):
        if axis == "z":
            return {"ra": ((z + j) % 4) * 4 + y}
        if axis == "y":
            return {"ra": z * 4 + (y + j) % 4}
        if axis == "x":
            return {"cb": (x + j) % 4}
        return {"dp": 1 - k}

    def rdma(src, dst, ss, rs, axis, j):
        return pltpu.make_async_remote_copy(
            src_ref=src, dst_ref=dst, send_sem=ss, recv_sem=rs, device_id=peer(axis, j), device_id_type=MESH
        )

    def cols(at):
        return pl.ds(pl.multiple_of(at * 256, 256), 256)

    phases = {
        "xz": (0, "z", lambda c, j: xg.at[c, x, :, cols(z)], lambda c, j: xg.at[c, x, :, cols(z)], lambda c, j: xg.at[c, x, :, cols((z + 4 - j) % 4)]),
        "xx": (1, "x", lambda c, j: xg.at[c, x], lambda c, j: xg.at[c, x], lambda c, j: xg.at[c, (x + 4 - j) % 4]),
        "yr": (2, "y", lambda c, j: ps.at[c, (y + j) % 4], lambda c, j: pr.at[c, j - 1], lambda c, j: pr.at[c, j - 1]),
        "ya": (3, "y", lambda c, j: hg.at[c, y], lambda c, j: hg.at[c, y], lambda c, j: hg.at[c, (y + 4 - j) % 4]),
        "zr": (4, "z", lambda c, j: os.at[c, (z + j) % 4], lambda c, j: zr.at[c, j - 1], lambda c, j: zr.at[c, j - 1]),
        "xr": (5, "x", lambda c, j: xs.at[c, (x + j) % 4], lambda c, j: xr.at[c, j - 1], lambda c, j: xr.at[c, j - 1]),
        "ez": (6, "z", lambda c, j: be.at[0, c], lambda c, j: be_in.at[0, c, j - 1], lambda c, j: be_in.at[0, c, j - 1]),
        "ey": (7, "y", lambda c, j: be.at[1, c], lambda c, j: be_in.at[1, c, j - 1], lambda c, j: be_in.at[1, c, j - 1]),
        "xo": (8, "x", lambda c, j: out.at[c, x], lambda c, j: out.at[c, x], lambda c, j: out.at[c, (x + 4 - j) % 4]),
    }

    def copy(name, c, j, landing=False):
        n, axis, src, dst, land = phases[name]
        return rdma(src(c, j), (land if landing else dst)(c, j), ssem.at[n, c, j - 1], rsem.at[n, c, j - 1], axis, j)

    def send(name, c):
        for j in (1, 3, 2):
            copy(name, c, j).start()

    def arrived(name, c):
        for j in (1, 3, 2):
            copy(name, c, j, True).wait_recv()

    def up_block(j):
        return rdma(
            up_hbm.at[pl.ds(pl.multiple_of(k * 128, 128), 128), pl.ds(pl.multiple_of(((z + j) % 4) * 1024, 1024), 1024)],
            wu.at[z, k], wssem.at[0, j - 1], wrsem.at[0, j - 1], "z", j,
        )

    def down_block(j):
        return rdma(
            down_hbm.at[pl.ds(pl.multiple_of(((z + j) % 4) * 1024 + k * 512, 512), 512), :],
            wd.at[z, k], wssem.at[1, j - 1], wrsem.at[1, j - 1], "z", j,
        )

    def got(w, n, j):
        at = w.at[(z + 4 - j) % 4, k]
        return rdma(at, at, wssem.at[n, j - 1], wrsem.at[n, j - 1], "z", j)

    def hand(w, n, j, half):
        at = w.at[(z + 4 - j) % 4, half]
        return rdma(at, at, wssem.at[n + 2, j - 1], wrsem.at[n + 2, j - 1], "k", 0)

    def e_copy(n, j):
        return rdma(e_own.at[n], e_in.at[n, j - 1], wssem.at[4 + n, j - 1], wrsem.at[4 + n, j - 1], "zy"[n], j)

    barrier = pltpu.get_barrier_semaphore()
    partners = [(axis, j) for axis in "xyz" for j in (1, 2, 3)] + [("k", 0)]
    for axis, j in partners:
        pl.semaphore_signal(barrier, inc=1, device_id=peer(axis, j), device_id_type=MESH)

    own = []
    for half in range(2):
        own.append(pltpu.make_async_copy(
            up_hbm.at[pl.ds(half * 128, 128), pl.ds(pl.multiple_of(z * 1024, 1024), 1024)], wu.at[z, half], lsem.at[half]))
        own.append(pltpu.make_async_copy(
            down_hbm.at[pl.ds(pl.multiple_of(z * 1024 + half * 512, 512), 512), :], wd.at[z, half], lsem.at[2 + half]))
    for o in own:
        o.start()

    gain = pre_gain[...]

    def scale(c, _):
        xg[c, x, :, cols(z)] = (tok[c, x].astype(f32) * gain).astype(bf16)
        return 0

    lax.fori_loop(0, C, scale, 0)
    pl.semaphore_wait(barrier, len(partners))

    send("xz", 0)
    for j in (1, 3, 2):
        up_block(j).start()
    lax.fori_loop(1, C, lambda c, _: (send("xz", c), 0)[1], 0)
    for j in (1, 3, 2):
        down_block(j).start()

    def own_energy(c, _):
        part = tok[c].reshape(R, 256).astype(f32)
        e_own[0, c] = lane_sums_as_row(part * part)
        return 0

    lax.fori_loop(0, C, own_energy, 0)
    for j in (1, 3, 2):
        e_copy(0, j).start()

    def relay(c, _):
        arrived("xz", c)
        send("xx", c)
        return 0

    relay(0, 0)
    for j in (1, 3, 2):
        got(wu, 0, j).wait_recv()
        hand(wu, 0, j, k).start()
    lax.fori_loop(1, C, relay, 0)
    for j in (1, 3, 2):
        e_copy(0, j).wait_recv()
    e_own[1] = e_own[0] + e_in[0, 0] + e_in[0, 1] + e_in[0, 2]
    for j in (1, 3, 2):
        e_copy(1, j).start()
    for j in (1, 3, 2):
        e_copy(1, j).wait_recv()
    for c in range(C):
        total = e_own[1, c] + e_in[1, 0, c] + e_in[1, 1, c] + e_in[1, 2, c]
        inverse = lax.rsqrt(total / D + epsilon)
        inv_col[c] = jnp.transpose(inverse).reshape(4, Q, 8)
    for o in own:
        o.wait()
    for j in (1, 3, 2):
        hand(wu, 0, j, 1 - k).wait_recv()

    def up(c):
        arrived("xx", c)
        rows = xg[c].reshape(R, 1024)
        for n in range(4):
            w = wu[:, :, :, n * 256 : (n + 1) * 256].reshape(1024, 256)
            part = jnp.dot(rows, w, preferred_element_type=f32)
            ps[c, :, :, n * 256 : (n + 1) * 256] = part.reshape(4, Q, 256).astype(bf16)
        send("yr", c)

    def activate(c):
        arrived("yr", c)
        inverse = inv_col[c, y][:, 0:1]
        for n in range(4):
            at = slice(n * 256, (n + 1) * 256)
            pre = ps[c, y, :, at].astype(f32)
            for j in range(3):
                pre = pre + pr[c, j, :, at].astype(f32)
            pre = pre * inverse + up_bias[z, :, at]
            hg[c, y, :, at] = jnp.square(jnp.maximum(pre, 0.0)).astype(bf16)
        send("ya", c)

    def down(c):
        arrived("ya", c)
        rows = hg[c].reshape(R, 1024)
        for n in range(4):
            os[c, n] = jnp.dot(rows, wd[n].reshape(1024, 256), preferred_element_type=f32).astype(bf16)
        send("zr", c)

    def sum_z(c):
        arrived("zr", c)
        total = os[c, z].astype(f32)
        for j in range(3):
            total = total + zr[c, j].astype(f32)
        xs[c] = total.reshape(4, Q, 256).astype(bf16)
        send("xr", c)

    def sum_x(c):
        arrived("xr", c)
        total = xs[c, x].astype(f32)
        for j in range(3):
            total = total + xr[c, j].astype(f32)
        br[c] = total
        be[0, c] = lane_sums_as_row(total * total)
        send("ez", c)

    def energy_y(c):
        arrived("ez", c)
        be[1, c] = be[0, c] + be_in[0, c, 0] + be_in[0, c, 1] + be_in[0, c, 2]
        send("ey", c)

    def finish(c):
        arrived("ey", c)
        total = be[1, c] + be_in[1, c, 0] + be_in[1, c, 1] + be_in[1, c, 2]
        inverse = jnp.transpose(lax.rsqrt(total / D + epsilon))[:, 0:1]
        normed = br[c] * inverse * post_gain[...]
        out[c, x] = (residual_weight * tok[c, x].astype(f32) + normed).astype(bf16)
        send("xo", c)

    stages = (up, activate, down, sum_z, sum_x, energy_y, finish)

    def step(s, _):
        for depth, stage in enumerate(stages):
            if depth == 2:
                @pl.when(s == 2)
                def _():
                    for j in (1, 3, 2):
                        got(wd, 1, j).wait_recv()
                        hand(wd, 1, j, k).start()
                    for j in (1, 3, 2):
                        hand(wd, 1, j, 1 - k).wait_recv()

            pl.when((s >= depth) & (s < C + depth))(lambda stage=stage, depth=depth: stage(s - depth))
        return 0

    lax.fori_loop(0, C + len(stages) - 1, step, 0)

    def close(c, _):
        arrived("xo", c)
        for name in phases:
            for j in (1, 2, 3):
                copy(name, c, j).wait_send()
        return 0

    lax.fori_loop(0, C, close, 0)
    for j in (1, 2, 3):
        up_block(j).wait_send()
        down_block(j).wait_send()
        hand(wu, 0, j, k).wait_send()
        hand(wd, 1, j, k).wait_send()
        e_copy(0, j).wait_send()
        e_copy(1, j).wait_send()


def body(tokens, pre_gain, up_weight, up_bias, down_weight, post_gain):
    C = CHUNKS
    T = tokens.shape[0]
    R = T // C
    Q = R // 4
    vmem = pl.BlockSpec(memory_space=pltpu.VMEM)
    hbm = pl.BlockSpec(memory_space=pl.ANY)
    dma = pltpu.SemaphoreType.DMA
    result = pl.pallas_call(
        kernel,
        out_shape=jax.ShapeDtypeStruct((C, 4, Q, 256), bf16),
        in_specs=[vmem, vmem, vmem, vmem, hbm, hbm],
        out_specs=vmem,
        scratch_shapes=[
            pltpu.VMEM((C, 4, Q, 1024), bf16),
            pltpu.VMEM((4, 2, 128, 1024), bf16),
            pltpu.VMEM((4, 2, 512, 256), bf16),
            pltpu.VMEM((C, 4, Q, 1024), bf16),
            pltpu.VMEM((C, 3, Q, 1024), bf16),
            pltpu.VMEM((C, 4, Q, 1024), bf16),
            pltpu.VMEM((C, 4, R, 256), bf16),
            pltpu.VMEM((C, 3, R, 256), bf16),
            pltpu.VMEM((C, 4, Q, 256), bf16),
            pltpu.VMEM((C, 3, Q, 256), bf16),
            pltpu.VMEM((C, Q, 256), f32),
            pltpu.VMEM((C, 4, Q, 8), f32),
            pltpu.VMEM((2, C, 8, R), f32),
            pltpu.VMEM((2, 3, C, 8, R), f32),
            pltpu.VMEM((2, C, 8, Q), f32),
            pltpu.VMEM((2, C, 3, 8, Q), f32),
            dma((9, C, 3)),
            dma((9, C, 3)),
            dma((6, 3)),
            dma((6, 3)),
            dma((4,)),
        ],
        compiler_params=pltpu.CompilerParams(
            collective_id=0, has_side_effects=True, vmem_limit_bytes=56 * 2**20
        ),
    )(
        tokens.reshape(C, 4, Q, 256),
        pre_gain.reshape(1, 256),
        up_bias.reshape(4, 1, 1024),
        post_gain.reshape(1, 256),
        up_weight,
        down_weight,
    )
    return result.reshape(T, 256)


def solution(mesh):
    in_specs = (P("dp", "ra"), P("ra"), P("ra", "cb"), P("cb"), P("cb", "ra"), P("ra"))
    out_specs = P("dp", "ra")
    return jax.shard_map(body, mesh=mesh, in_specs=in_specs, out_specs=out_specs, check_vma=False)
```

time: 353 us -> 149 us (0.42)
  waiting for transfers between devices: 279 us -> 0 us
  Pallas kernels: 0 us -> 147 us
  blocking collectives: 30.1 us -> 0 us
  matrix products: 21.1 us -> 0 us
  between operations: 13.2 us -> 0.01 us
  other arithmetic: 7.27 us -> 0 us
    pallas_call x0 -> x1, Pallas kernels: none -> 147 us  [body(): pl.pallas_call(kernel, out_shape=jax.ShapeDtypeStruct((C, 4, Q, 256), bf1...]
    reduce_scatter x1 -> x0, waiting for transfers between devices: 139 us -> none  [body(): lax.psum_scatter(partial_value, 'ra', scatter_dimension=0, tiled=True)]
    all_gather x1 -> x0, waiting for transfers between devices: 89.6 us -> none  [body(): lax.all_gather(hidden, 'ra', axis=0, tiled=True)]
    psum x1 -> x0, waiting for transfers between devices: 50.1 us -> none  [body(): branch = lax.psum(branch, 'cb')]
    all_to_all x2 -> x0, blocking collectives: 30.1 us -> none  [the longest x1 15.5 us: sent_and_summed(): pieces = lax.all_to_all(in_blocks(array, dim, size), axis, 0, 0, tiled=True)]
    dot_general x2 -> x0, matrix products: 21.1 us -> none  [the longest x1 11.2 us: body(): jnp.dot(scaled, up_weight, preferred_element_type=jnp.float32)]
    convert_element_type x2 -> x0, other arithmetic: 5.2 us -> none  [the longest x1 2.61 us: body(): return (residual_weight * stream + normed).astype(jnp.bfloat16)]
  transfers between devices with their start and end apart: 3 -> 0, of which waited for: 3 -> 0; matrix products, arithmetic and copies ran while one was open for 0% -> 0% of each run, Pallas kernels for 0% -> 0%
where the time goes in v1:
time: 149 us
  Pallas kernels  147 us (99%)
  local copies, waits for them, and re-layouts  2.06 us (1%)
    pallas_call x1, Pallas kernels, body(): pl.pallas_call(kernel, out_shape=jax.ShapeDtypeStruct((C, 4, Q, 256), bf1...  147 us

profile of v1, /device:TPU:0, one launch (start us, length us, event | category | flops | bytes accessed | tf_op | source)
XLA Modules:
  0.0 149.0 jit_solution(7349046223985260976)
XLA Ops:
  0.0 146.9 %shard_map.64 = bf16[6,4,64,256]{3,2,1,0:T(8,128)(2,1)} custom-call(bf16[6,4,64,256]{3,2,1,0:T(8,128)(2,1)} %bitcast.6, f32[1,256]{1,0:T(1,128)} %bitcast.8, f32[4,1,1024]{2,1,0:T(1,128)} %bitcast.7, f32[1,256]{1,0:T(1,128)} %bitcast.9, bf16[256,4096]{1,0:T(8,128)(2,1)} %up_hbm.1, bf16[4096,256]{1,0:T(8,128)(2,1)} %down_hbm.1), custom_call_target="tpu_custom_call" | custom-call | tf_op jit(solution)/shard_map/pallas_call | solution.py:268
  146.9 2.1 %copy.8 = bf16[1536,256]{1,0:T(8,128)(2,1)} copy(bf16[1536,256]{1,0:T(8,128)(2,1)} %bitcast.5) | data formatting | bytes 1572864

commit v2 on v0

v2 whole, which is shorter than its diff:
```python
import jax
import jax.numpy as jnp
from jax import lax
from jax.experimental import pallas as pl
from jax.experimental.pallas import tpu as pltpu
from jax.sharding import PartitionSpec as P

MESH = pl.DeviceIdType.MESH
D = 4096
CHUNKS = 12
GROUP = 4
LAG = 2
LATER = (4, 4, 6)
VMEM_LIMIT = 56 * 2**20
epsilon = 1e-06
residual_weight = 0.5
f32, bf16 = jnp.float32, jnp.bfloat16


def lane_sums_as_row(square):
    ones = jnp.ones((8, square.shape[1]), bf16)
    high = square.astype(bf16)
    low = (square - high.astype(f32)).astype(bf16)
    contract = (((1,), (1,)), ((), ()))
    total = lax.dot_general(ones, high, contract, preferred_element_type=f32)
    return total + lax.dot_general(ones, low, contract, preferred_element_type=f32)


def kernel(
    tok_hbm, pre_gain, up_bias, post_gain, up_hbm, down_hbm, out_hbm,
    tok, xg, wu, wd, pf, ps, r1, rs, pr, hg, os, of, zr, xa, inv_row, inv_col, e_own, e_in, be, be_in, out,
    ssem, csem, usem, esem, wssem, wrsem, lsem, osem,
):
    G = GROUP
    C, _, Q, _ = tok.shape
    R = 4 * Q
    ra, x, k = lax.axis_index("ra"), lax.axis_index("cb"), lax.axis_index("dp")
    z, y = ra // 4, ra % 4
    halves = (slice(0, 256), slice(256, 512))

    def peer(axis, j):
        if axis == "r":
            return {"ra": (ra + j) % 16}
        if axis == "z":
            return {"ra": ((z + j) % 4) * 4 + y}
        if axis == "y":
            return {"ra": z * 4 + (y + j) % 4}
        if axis == "x":
            return {"cb": (x + j) % 4}
        return {"dp": 1 - k}

    def rdma(src, dst, ss, rs, axis, j):
        return pltpu.make_async_remote_copy(
            src_ref=src, dst_ref=dst, send_sem=ss, recv_sem=rs, device_id=peer(axis, j), device_id_type=MESH
        )

    def cols(at):
        return pl.ds(pl.multiple_of(at * 256, 256), 256)

    def side(j):
        return 0 if j == 1 else 1

    phases = {
        "xz": (0, "z", (1, 3, 2), lambda c, j: xg.at[c, x, :, cols(z)], lambda c, j: xg.at[c, x, :, cols(z)],
               lambda c: xa.at[c, 0:3, 0:Q]),
        "xx": (1, "x", (1, 3, 2), lambda c, j: xg.at[c, x], lambda c, j: xg.at[c, x], lambda c: xg.at[c, 0:3]),
        "r1": (2, "y", (1, 3), lambda u, j: ps.at[u, (y + 2) % 4, :, halves[side(j)]], lambda u, j: r1.at[u, side(j)],
               lambda u: r1.at[u]),
        "rd": (3, "y", (1, 3), lambda u, j: ps.at[u, (y + j) % 4, :, halves[1 - side(j)]],
               lambda u, j: pr.at[u, side(j), :, halves[1 - side(j)]], lambda u: r1.at[u]),
        "r2": (4, "y", (1, 3), lambda u, j: rs.at[u, side(j)], lambda u, j: pr.at[u, side(j), :, halves[side(j)]],
               lambda u: pr.at[u]),
        "a1": (5, "y", (1, 3), lambda u, j: hg.at[u, y], lambda u, j: hg.at[u, y], lambda u: hg.at[u, 0:2]),
        "a2": (6, "y", (1, 3), lambda u, j: hg.at[u, (y + 4 - j) % 4, :, halves[side(j)]],
               lambda u, j: hg.at[u, (y + 4 - j) % 4, :, halves[side(j)]], lambda u: r1.at[u]),
        "zr": (7, "z", (1, 3, 2), lambda c, j: os.at[c, (z + j) % 4], lambda c, j: zr.at[c, j - 1], lambda c: zr.at[c]),
        "xa": (8, "x", (1, 3, 2), lambda c, j: xa.at[c, x], lambda c, j: xa.at[c, x], lambda c: zr.at[c]),
    }
    sent = {
        "xz": xa.at[:, 0:3, 0:Q], "xx": xg.at[:, 0:3], "r1": r1, "rd": r1, "r2": r1, "a1": hg.at[:, 0:2], "a2": r1, "zr": zr,
        "xa": zr,
    }
    by_chunk = {"xz": 0, "xx": 1, "zr": 2, "xa": 3}
    by_unit = {"r1": 0, "rd": 1, "r2": 1, "a1": 2, "a2": 3}

    def landed(name, i):
        return csem.at[by_chunk[name], i] if name in by_chunk else usem.at[by_unit[name], i]

    def send(name, i):
        n, axis, offsets, src, dst, _ = phases[name]
        for j in offsets:
            rdma(src(i, j), dst(i, j), ssem.at[n], landed(name, i), axis, j).start()

    def arrived(name, i):
        with jax.named_scope("wait_" + name):
            all_of_it = phases[name][5](i)
            pltpu.make_async_copy(all_of_it, all_of_it, landed(name, i)).wait()

    def up_block(h, j):
        at = pl.ds(pl.multiple_of(((z + j) % 4) * 1024 + h * 512, 512), 512)
        return rdma(
            up_hbm.at[pl.ds(pl.multiple_of(k * 128, 128), 128), at], wu.at[h, z, k], wssem.at[h], wrsem.at[h, j - 1], "z", j
        )

    def down_block(j):
        return rdma(
            down_hbm.at[pl.ds(pl.multiple_of(((z + j) % 4) * 1024 + k * 512, 512), 512), :],
            wd.at[z, k], wssem.at[2], wrsem.at[2, j - 1], "z", j,
        )

    def got(w, n, j):
        at = w.at[(z + 4 - j) % 4, k]
        return rdma(at, at, wssem.at[n], wrsem.at[n, j - 1], "z", j)

    def hand(w, n, j, half):
        at = w.at[(z + 4 - j) % 4, half]
        return rdma(at, at, wssem.at[n + 3], wrsem.at[n + 3, j - 1], "k", 0)

    def take(w, n):
        with jax.named_scope("wait_w"):
            for j in (1, 3, 2):
                got(w, n, j).wait_recv()
                hand(w, n, j, k).start()

    def have(w, n):
        with jax.named_scope("wait_hand"):
            for j in (1, 3, 2):
                hand(w, n, j, 1 - k).wait_recv()

    def send_energy(n):
        for j in (1, 3, 2):
            rdma(e_own.at[n], e_in.at[n, j - 1], esem.at[n], esem.at[2 + n], "zy"[n], j).start()

    def have_energy(n):
        with jax.named_scope("wait_e"):
            pltpu.make_async_copy(e_in.at[n], e_in.at[n], esem.at[2 + n]).wait()
        return e_own[n] + e_in[n, 0] + e_in[n, 1] + e_in[n, 2]

    def send_rows(c):
        for j in range(1, 16):
            rdma(be.at[c], be_in.at[c, j - 1], esem.at[4], esem.at[5 + c], "r", j).start()

    load = pltpu.make_async_copy(tok_hbm, tok, lsem.at[6])
    load.start()
    barrier = pltpu.get_barrier_semaphore()
    partners = [(axis, j) for axis in "xyz" for j in (1, 2, 3)] + [("k", 0)]
    for axis, j in partners:
        pl.semaphore_signal(barrier, inc=1, device_id=peer(axis, j), device_id_type=MESH)

    own = []
    for half in range(2):
        for h in range(2):
            own.append(pltpu.make_async_copy(
                up_hbm.at[pl.ds(half * 128, 128), pl.ds(pl.multiple_of(z * 1024 + h * 512, 512), 512)],
                wu.at[h, z, half], lsem.at[half * 2 + h]))
        own.append(pltpu.make_async_copy(
            down_hbm.at[pl.ds(pl.multiple_of(z * 1024 + half * 512, 512), 512), :], wd.at[z, half], lsem.at[4 + half]))
    for o in own:
        o.start()
    load.wait()

    gain = pre_gain[...]

    def scale(c, _):
        xg[c, x, :, cols(z)] = (tok[c, x].astype(f32) * gain).astype(bf16)
        part = tok[c].reshape(R, 256).astype(f32)
        e_own[0, c] = lane_sums_as_row(part * part)[0:1]
        return 0

    with jax.named_scope("scale"):
        lax.fori_loop(0, C, scale, 0)
    with jax.named_scope("wait_barrier"):
        pl.semaphore_wait(barrier, len(partners))

    early = max(G, C // 2)
    for c in range(2):
        send("xz", c)
    for j in (1, 3, 2):
        up_block(0, j).start()
    send_energy(0)
    for c in range(2, early):
        send("xz", c)
    for j in (1, 3, 2):
        up_block(1, j).start()
    lax.fori_loop(early, C, lambda c, _: (send("xz", c), 0)[1], 0)
    for j in (1, 3, 2):
        down_block(j).start()

    def spread(c):
        arrived("xz", c)
        send("xx", c)

    spread(0)
    spread(1)
    take(wu.at[0], 0)
    for o in own:
        o.wait()
    have(wu.at[0], 0)

    def energy_over_z():
        e_own[1] = have_energy(0)
        send_energy(1)

    def energy_over_y():
        inv_row[...] = lax.rsqrt(have_energy(1) / D + epsilon)

        def turn(c, _):
            inv_col[c] = jnp.transpose(jnp.broadcast_to(inv_row[c], (8, R))).reshape(4, Q, 8)
            return 0

        lax.fori_loop(0, C, turn, 0)

    def late(u):
        return (u // (2 * G) + 15) // 16

    def chunk_of(u):
        return late(u) * (u // 2) + (1 - late(u)) * (u % G)

    def half_of(u):
        return late(u) * (u % 2) + (1 - late(u)) * (u // G)

    def up(u):
        c, h = chunk_of(u), half_of(u)
        rows = xg[c].reshape(R, 1024)
        for n in range(2):
            at = slice(n * 256, (n + 1) * 256)
            part = jnp.dot(rows, wu[h, :, :, :, at].reshape(1024, 256), preferred_element_type=f32).reshape(4, Q, 256)
            pf[u, :, :, at] = part
            ps[u, :, :, at] = part.astype(bf16)
        send("r1", u)
        send("rd", u)

    def add_up(u):
        arrived("r1", u)
        for j in (1, 3):
            n = side(j)
            rs[u, n] = (pf[u, (y + j) % 4, :, halves[n]] + r1[u, n].astype(f32)).astype(bf16)
        send("r2", u)

    def activate(u):
        arrived("r2", u)
        inverse = inv_col[chunk_of(u), y][:, 0:1]
        pre = pf[u, y] + pr[u, 0].astype(f32) + pr[u, 1].astype(f32)
        pre = pre * inverse + up_bias[z, half_of(u)]
        hg[u, y] = jnp.square(jnp.maximum(pre, 0.0)).astype(bf16)
        send("a1", u)

    def pass_on(u):
        arrived("a1", u)
        send("a2", u)

    def last_of(u):
        return late(u) * ((u - 1) // 2) + (1 - late(u)) * (u - G)

    def down(u):
        c = last_of(u)
        other = late(u) * (u - 1) + (1 - late(u)) * (u - G)
        for n in range(4):
            part = jnp.dot(hg[other].reshape(R, 512), wd[n, 0], preferred_element_type=f32)
            part = part + jnp.dot(hg[u].reshape(R, 512), wd[n, 1], preferred_element_type=f32)
            of[c, n] = part
            os[c, n] = part.astype(bf16)
        send("zr", c)

    def sum_z(u):
        c = last_of(u)
        arrived("zr", c)
        total = of[c, z]
        for j in range(3):
            total = total + zr[c, j].astype(f32)
        xa[c, x] = total.astype(bf16)
        send("xa", c)

    def branch(c):
        return (xa[c, 0].astype(f32) + xa[c, 1].astype(f32)) + (xa[c, 2].astype(f32) + xa[c, 3].astype(f32))

    def sum_x(u):
        c = last_of(u)
        arrived("xa", c)
        total = branch(c)
        be[c] = lane_sums_as_row(total * total)[0:1]
        send_rows(c)

    def finish(u):
        c = last_of(u)
        with jax.named_scope("wait_be"):
            pltpu.make_async_copy(be_in.at[c], be_in.at[c], esem.at[5 + c]).wait()
        total = be[c]
        for j in range(15):
            total = total + be_in[c, j]
        inverse = jnp.transpose(jnp.broadcast_to(lax.rsqrt(total / D + epsilon), (8, R)))[:, 0:1]
        normed = branch(c) * inverse * post_gain[...]
        out[c] = (residual_weight * tok[c].reshape(R, 256).astype(f32) + normed).astype(bf16)
        pltpu.make_async_copy(out.at[c], out_hbm.at[c], osem.at[c]).start()

    def scoped(stage, u):
        with jax.named_scope(stage.__name__):
            stage(u)

    lag = LAG
    to_down = 4 * lag
    to_z = to_down + LATER[0]
    to_x = to_z + LATER[1]
    to_end = to_x + LATER[2]

    def step(s, _):
        def at(stage, depth, ends=False):
            u = s - depth
            now = (u >= 0) & (u < 2 * C)
            if ends:
                now = now & (u >= G) & ((u < 2 * G) | (u % 2 == 1))
            pl.when(now)(lambda: scoped(stage, u))

        pl.when((s < 2 * C) & ((s < G) | ((s >= 2 * G) & (s % 2 == 0))))(lambda: arrived("xx", chunk_of(s)))
        pl.when(s == G)(lambda: have(wu.at[1], 1))
        at(up, 0)
        pl.when((s + 2 < early))(lambda: scoped(spread, s + 2))
        pl.when(s == lag)(energy_over_z)
        at(add_up, lag)
        pl.when(s == G - 1)(lambda: take(wu.at[1], 1))
        pl.when(s == 2 * lag)(energy_over_y)
        at(activate, 2 * lag)
        pl.when((s >= early) & (s < C))(lambda: scoped(spread, s))
        at(pass_on, 3 * lag)
        pl.when(s == G + to_down - 1)(lambda: take(wd, 2))
        pl.when(s == G + to_down)(lambda: have(wd, 2))
        pl.when((s >= to_down) & (s < 2 * C + to_down))(lambda: arrived("a2", s - to_down))
        at(down, to_down, True)
        at(sum_z, to_z, True)
        at(sum_x, to_x, True)
        at(finish, to_end, True)
        return 0

    lax.fori_loop(0, 2 * C + to_end, step, 0)
    with jax.named_scope("sent"):
        for name, total in sent.items():
            pltpu.make_async_copy(total, total, ssem.at[phases[name][0]]).wait()
        some = wu.at[0, 0:3, 0]
        for n, total in enumerate((some, some, wd.at[0:3, 0], some, some, wd.at[0:3, 0])):
            pltpu.make_async_copy(total, total, wssem.at[n]).wait()
        for n in range(2):
            pltpu.make_async_copy(e_in.at[n], e_in.at[n], esem.at[n]).wait()
        pltpu.make_async_copy(be_in, be_in, esem.at[4]).wait()
        lax.fori_loop(0, C, lambda c, _: (pltpu.make_async_copy(out.at[c], out_hbm.at[c], osem.at[c]).wait(), 0)[1], 0)


def body(tokens, pre_gain, up_weight, up_bias, down_weight, post_gain):
    C = CHUNKS
    T = tokens.shape[0]
    R = T // C
    Q = R // 4
    vmem = pl.BlockSpec(memory_space=pltpu.VMEM)
    hbm = pl.BlockSpec(memory_space=pl.ANY)
    dma = pltpu.SemaphoreType.DMA
    result = pl.pallas_call(
        kernel,
        out_shape=jax.ShapeDtypeStruct((C, R, 256), bf16),
        in_specs=[hbm, vmem, vmem, vmem, hbm, hbm],
        out_specs=hbm,
        scratch_shapes=[
            pltpu.VMEM((C, 4, Q, 256), bf16),
            pltpu.VMEM((C, 4, Q, 1024), bf16),
            pltpu.VMEM((2, 4, 2, 128, 512), bf16),
            pltpu.VMEM((4, 2, 512, 256), bf16),
            pltpu.VMEM((2 * C, 4, Q, 512), f32),
            pltpu.VMEM((2 * C, 4, Q, 512), bf16),
            pltpu.VMEM((2 * C, 2, Q, 256), bf16),
            pltpu.VMEM((2 * C, 2, Q, 256), bf16),
            pltpu.VMEM((2 * C, 2, Q, 512), bf16),
            pltpu.VMEM((2 * C, 4, Q, 512), bf16),
            pltpu.VMEM((C, 4, R, 256), bf16),
            pltpu.VMEM((C, 4, R, 256), f32),
            pltpu.VMEM((C, 3, R, 256), bf16),
            pltpu.VMEM((C, 4, R, 256), bf16),
            pltpu.VMEM((C, 1, R), f32),
            pltpu.VMEM((C, 4, Q, 8), f32),
            pltpu.VMEM((2, C, 1, R), f32),
            pltpu.VMEM((2, 3, C, 1, R), f32),
            pltpu.VMEM((C, 1, R), f32),
            pltpu.VMEM((C, 15, 1, R), f32),
            pltpu.VMEM((C, R, 256), bf16),
            dma((9,)),
            dma((4, C)),
            dma((4, 2 * C)),
            dma((5 + C,)),
            dma((6,)),
            dma((6, 3)),
            dma((7,)),
            dma((C,)),
        ],
        compiler_params=pltpu.CompilerParams(
            collective_id=0, has_side_effects=True, vmem_limit_bytes=VMEM_LIMIT
        ),
    )(
        tokens.reshape(C, 4, Q, 256),
        pre_gain.reshape(1, 256),
        up_bias.reshape(4, 2, 1, 512),
        post_gain.reshape(1, 256),
        up_weight,
        down_weight,
    )
    return result.reshape(T, 256)


def solution(mesh):
    in_specs = (P("dp", "ra"), P("ra"), P("ra", "cb"), P("cb"), P("cb", "ra"), P("ra"))
    out_specs = P("dp", "ra")
    return jax.shard_map(body, mesh=mesh, in_specs=in_specs, out_specs=out_specs, check_vma=False)
```

time: 353 us -> 105 us (0.30)
  waiting for transfers between devices: 279 us -> 0 us
  Pallas kernels: 0 us -> 102 us
  blocking collectives: 30.1 us -> 0 us
  matrix products: 21.1 us -> 0 us
  between operations: 13.2 us -> 0.01 us
  other arithmetic: 7.27 us -> 0 us
    reduce_scatter x1 -> x0, waiting for transfers between devices: 139 us -> none  [body(): lax.psum_scatter(partial_value, 'ra', scatter_dimension=0, tiled=True)]
    pallas_call x0 -> x1, Pallas kernels: none -> 102 us  [body(): pl.pallas_call(kernel, out_shape=jax.ShapeDtypeStruct((C, R, 256), bf16),...]
    all_gather x1 -> x0, waiting for transfers between devices: 89.6 us -> none  [body(): lax.all_gather(hidden, 'ra', axis=0, tiled=True)]
    psum x1 -> x0, waiting for transfers between devices: 50.1 us -> none  [body(): branch = lax.psum(branch, 'cb')]
    all_to_all x2 -> x0, blocking collectives: 30.1 us -> none  [the longest x1 15.5 us: sent_and_summed(): pieces = lax.all_to_all(in_blocks(array, dim, size), axis, 0, 0, tiled=True)]
    dot_general x2 -> x0, matrix products: 21.1 us -> none  [the longest x1 11.2 us: body(): jnp.dot(scaled, up_weight, preferred_element_type=jnp.float32)]
    convert_element_type x2 -> x0, other arithmetic: 5.2 us -> none  [the longest x1 2.61 us: body(): return (residual_weight * stream + normed).astype(jnp.bfloat16)]
  transfers between devices with their start and end apart: 3 -> 0, of which waited for: 3 -> 0; matrix products, arithmetic and copies ran while one was open for 0% -> 0% of each run, Pallas kernels for 0% -> 0%
where the time goes in v2:
time: 105 us
  Pallas kernels  102 us (97%)
  local copies, waits for them, and re-layouts  2.06 us (2%)
    pallas_call x1, Pallas kernels, body(): pl.pallas_call(kernel, out_shape=jax.ShapeDtypeStruct((C, R, 256), bf16),...  102 us

profile of v2, /device:TPU:0, one launch (start us, length us, event | category | flops | bytes accessed | tf_op | source)
XLA Modules:
  0.0 104.5 jit_solution(6712949851001953550)
XLA Ops:
  0.0 102.4 %shard_map.64 = bf16[12,128,256]{2,1,0:T(8,128)(2,1)} custom-call(bf16[12,4,32,256]{3,2,1,0:T(8,128)(2,1)} %bitcast.6, f32[1,256]{1,0:T(1,128)} %bitcast.8, f32[4,2,1,512]{3,2,1,0:T(1,128)} %bitcast.7, f32[1,256]{1,0:T(1,128)} %bitcast.9, bf16[256,4096]{1,0:T(8,128)(2,1)} %up_hbm.1, bf16[4096,256]{1,0:T(8,128)(2,1)} %down_hbm.1), custom_call_target="tpu_custom_call" | custom-call | tf_op jit(solution)/shard_map/pallas_call | solution.py:355
  102.5 2.1 %copy.8 = bf16[1536,256]{1,0:T(8,128)(2,1)} copy(bf16[1536,256]{1,0:T(8,128)(2,1)} %bitcast.5) | data formatting | bytes 1572864

commit v3 on v2

--- a/solution.py
+++ b/solution.py
@@ -8,8 +8,11 @@
 MESH = pl.DeviceIdType.MESH
 D = 4096
 CHUNKS = 12
-GROUP = 4
-LAG = 2
+GROUP = 5
+FIRST = 5
+AHEAD = 2
+EAGER = 5
+LAGS = (2, 2, 2, 2)
 LATER = (4, 4, 6)
 VMEM_LIMIT = 56 * 2**20
 epsilon = 1e-06
@@ -27,8 +30,8 @@
 
 
 def kernel(
-    tok_hbm, pre_gain, up_bias, post_gain, up_hbm, down_hbm, out_hbm,
-    tok, xg, wu, wd, pf, ps, r1, rs, pr, hg, os, of, zr, xa, inv_row, inv_col, e_own, e_in, be, be_in, out,
+    tok_hbm, pre_gain_hbm, up_bias_hbm, post_gain_hbm, up_hbm, down_hbm, out_hbm,
+    tok, pre_gain, up_bias, post_gain, xg, wu, wd, pf, ps, r1, rs, pr, hg, os, of, zr, xa, inv_row, inv_col, e_own, e_in, be, be_in, out,
     ssem, csem, usem, esem, wssem, wrsem, lsem, osem,
 ):
     G = GROUP
@@ -37,6 +40,7 @@
     ra, x, k = lax.axis_index("ra"), lax.axis_index("cb"), lax.axis_index("dp")
     z, y = ra // 4, ra % 4
     halves = (slice(0, 256), slice(256, 512))
+    wide = (slice(0, 512), slice(512, 1024))
 
     def peer(axis, j):
         if axis == "r":
@@ -63,7 +67,9 @@
     phases = {
         "xz": (0, "z", (1, 3, 2), lambda c, j: xg.at[c, x, :, cols(z)], lambda c, j: xg.at[c, x, :, cols(z)],
                lambda c: xa.at[c, 0:3, 0:Q]),
-        "xx": (1, "x", (1, 3, 2), lambda c, j: xg.at[c, x], lambda c, j: xg.at[c, x], lambda c: xg.at[c, 0:3]),
+        "xx": (1, "x", (1, 3), lambda c, j: xg.at[c, x], lambda c, j: xg.at[c, x], lambda c: xg.at[c, 0:2]),
+        "xf": (9, "x", (1, 3), lambda c, j: xg.at[c, (x + 4 - j) % 4, :, wide[side(j)]],
+               lambda c, j: xg.at[c, (x + 4 - j) % 4, :, wide[side(j)]], lambda c: xg.at[c, 0]),
         "r1": (2, "y", (1, 3), lambda u, j: ps.at[u, (y + 2) % 4, :, halves[side(j)]], lambda u, j: r1.at[u, side(j)],
                lambda u: r1.at[u]),
         "rd": (3, "y", (1, 3), lambda u, j: ps.at[u, (y + j) % 4, :, halves[1 - side(j)]],
@@ -77,11 +83,11 @@
         "xa": (8, "x", (1, 3, 2), lambda c, j: xa.at[c, x], lambda c, j: xa.at[c, x], lambda c: zr.at[c]),
     }
     sent = {
-        "xz": xa.at[:, 0:3, 0:Q], "xx": xg.at[:, 0:3], "r1": r1, "rd": r1, "r2": r1, "a1": hg.at[:, 0:2], "a2": r1, "zr": zr,
-        "xa": zr,
+        "xz": xa.at[:, 0:3, 0:Q], "xx": xg.at[:, 0:2], "xf": xg.at[:, 0], "r1": r1, "rd": r1, "r2": r1, "a1": hg.at[:, 0:2],
+        "a2": r1, "zr": zr, "xa": zr,
     }
-    by_chunk = {"xz": 0, "xx": 1, "zr": 2, "xa": 3}
-    by_unit = {"r1": 0, "rd": 1, "r2": 1, "a1": 2, "a2": 3}
+    by_chunk = {"xz": 0, "xx": 1, "zr": 2, "xa": 3, "xf": 4}
+    by_unit = {"r1": 0, "rd": 1, "r2": 1, "a1": 0, "a2": 1}
 
     def landed(name, i):
         return csem.at[by_chunk[name], i] if name in by_chunk else usem.at[by_unit[name], i]
@@ -140,13 +146,17 @@
         for j in range(1, 16):
             rdma(be.at[c], be_in.at[c, j - 1], esem.at[4], esem.at[5 + c], "r", j).start()
 
-    load = pltpu.make_async_copy(tok_hbm, tok, lsem.at[6])
-    load.start()
     barrier = pltpu.get_barrier_semaphore()
     partners = [(axis, j) for axis in "xyz" for j in (1, 2, 3)] + [("k", 0)]
     for axis, j in partners:
         pl.semaphore_signal(barrier, inc=1, device_id=peer(axis, j), device_id_type=MESH)
 
+    load = pltpu.make_async_copy(tok_hbm, tok, lsem.at[6])
+    load.start()
+    small = []
+    for n, (far, near) in enumerate(((pre_gain_hbm, pre_gain), (up_bias_hbm, up_bias), (post_gain_hbm, post_gain))):
+        small.append(pltpu.make_async_copy(far, near, lsem.at[7 + n]))
+        small[-1].start()
     own = []
     for half in range(2):
         for h in range(2):
@@ -158,11 +168,16 @@
     for o in own:
         o.start()
     load.wait()
+    for o in small:
+        o.wait()
 
     gain = pre_gain[...]
 
     def scale(c, _):
         xg[c, x, :, cols(z)] = (tok[c, x].astype(f32) * gain).astype(bf16)
+        return 0
+
+    def own_energy(c, _):
         part = tok[c].reshape(R, 256).astype(f32)
         e_own[0, c] = lane_sums_as_row(part * part)[0:1]
         return 0
@@ -173,12 +188,14 @@
         pl.semaphore_wait(barrier, len(partners))
 
     early = max(G, C // 2)
-    for c in range(2):
+    for c in range(FIRST):
         send("xz", c)
     for j in (1, 3, 2):
         up_block(0, j).start()
+    with jax.named_scope("own_energy"):
+        lax.fori_loop(0, C, own_energy, 0)
     send_energy(0)
-    for c in range(2, early):
+    for c in range(FIRST, early):
         send("xz", c)
     for j in (1, 3, 2):
         up_block(1, j).start()
@@ -190,9 +207,19 @@
         arrived("xz", c)
         send("xx", c)
 
-    spread(0)
-    spread(1)
+    def forward(c):
+        arrived("xx", c)
+        send("xf", c)
+
+    for c in range(FIRST):
+        spread(c)
+    for c in range(AHEAD):
+        forward(c)
     take(wu.at[0], 0)
+    for c in range(FIRST, G):
+        spread(c)
+    for c in range(AHEAD, EAGER):
+        forward(c)
     for o in own:
         o.wait()
     have(wu.at[0], 0)
@@ -204,11 +231,9 @@
     def energy_over_y():
         inv_row[...] = lax.rsqrt(have_energy(1) / D + epsilon)
 
-        def turn(c, _):
-            inv_col[c] = jnp.transpose(jnp.broadcast_to(inv_row[c], (8, R))).reshape(4, Q, 8)
-            return 0
-
-        lax.fori_loop(0, C, turn, 0)
+
+    def turn(c):
+        inv_col[c] = jnp.transpose(jnp.broadcast_to(inv_row[c], (8, R))).reshape(4, Q, 8)
 
     def late(u):
         return (u // (2 * G) + 15) // 16
@@ -291,14 +316,16 @@
         inverse = jnp.transpose(jnp.broadcast_to(lax.rsqrt(total / D + epsilon), (8, R)))[:, 0:1]
         normed = branch(c) * inverse * post_gain[...]
         out[c] = (residual_weight * tok[c].reshape(R, 256).astype(f32) + normed).astype(bf16)
-        pltpu.make_async_copy(out.at[c], out_hbm.at[c], osem.at[c]).start()
+        pltpu.make_async_copy(out.at[c], out_hbm.at[c], osem.at[0]).start()
 
     def scoped(stage, u):
         with jax.named_scope(stage.__name__):
             stage(u)
 
-    lag = LAG
-    to_down = 4 * lag
+    to_add = LAGS[0]
+    to_act = to_add + LAGS[1]
+    to_pass = to_act + LAGS[2]
+    to_down = to_pass + LAGS[3]
     to_z = to_down + LATER[0]
     to_x = to_z + LATER[1]
     to_end = to_x + LATER[2]
@@ -311,17 +338,21 @@
                 now = now & (u >= G) & ((u < 2 * G) | (u % 2 == 1))
             pl.when(now)(lambda: scoped(stage, u))
 
-        pl.when((s < 2 * C) & ((s < G) | ((s >= 2 * G) & (s % 2 == 0))))(lambda: arrived("xx", chunk_of(s)))
+        pl.when((s < 2 * C) & ((s < G) | ((s >= 2 * G) & (s % 2 == 0))))(lambda: arrived("xf", chunk_of(s)))
         pl.when(s == G)(lambda: have(wu.at[1], 1))
         at(up, 0)
-        pl.when((s + 2 < early))(lambda: scoped(spread, s + 2))
-        pl.when(s == lag)(energy_over_z)
-        at(add_up, lag)
-        pl.when(s == G - 1)(lambda: take(wu.at[1], 1))
-        pl.when(s == 2 * lag)(energy_over_y)
-        at(activate, 2 * lag)
+        pl.when(s + G < early)(lambda: scoped(spread, s + G))
+        at(add_up, to_add)
+        pl.when(s == 2)(energy_over_y)
+        pl.when(s == G - 2)(lambda: take(wu.at[1], 1))
+        v = s - to_act
+        pl.when((v < 2 * C) & (((v >= 0) & (v < G)) | ((v >= 2 * G) & (v % 2 == 0))))(lambda: turn(chunk_of(v)))
+        at(activate, to_act)
+        pl.when((s + 1 >= EAGER) & (s + 1 < G))(lambda: scoped(forward, s + 1))
+        pl.when((s >= G) & (s < early))(lambda: scoped(forward, s))
+        pl.when((s >= early + 3) & (s < C + 3))(lambda: scoped(forward, s - 3))
         pl.when((s >= early) & (s < C))(lambda: scoped(spread, s))
-        at(pass_on, 3 * lag)
+        at(pass_on, to_pass)
         pl.when(s == G + to_down - 1)(lambda: take(wd, 2))
         pl.when(s == G + to_down)(lambda: have(wd, 2))
         pl.when((s >= to_down) & (s < 2 * C + to_down))(lambda: arrived("a2", s - to_down))
@@ -331,6 +362,7 @@
         at(finish, to_end, True)
         return 0
 
+    energy_over_z()
     lax.fori_loop(0, 2 * C + to_end, step, 0)
     with jax.named_scope("sent"):
         for name, total in sent.items():
@@ -341,7 +373,7 @@
         for n in range(2):
             pltpu.make_async_copy(e_in.at[n], e_in.at[n], esem.at[n]).wait()
         pltpu.make_async_copy(be_in, be_in, esem.at[4]).wait()
-        lax.fori_loop(0, C, lambda c, _: (pltpu.make_async_copy(out.at[c], out_hbm.at[c], osem.at[c]).wait(), 0)[1], 0)
+        pltpu.make_async_copy(out, out_hbm, osem.at[0]).wait()
 
 
 def body(tokens, pre_gain, up_weight, up_bias, down_weight, post_gain):
@@ -349,16 +381,18 @@
     T = tokens.shape[0]
     R = T // C
     Q = R // 4
-    vmem = pl.BlockSpec(memory_space=pltpu.VMEM)
     hbm = pl.BlockSpec(memory_space=pl.ANY)
     dma = pltpu.SemaphoreType.DMA
     result = pl.pallas_call(
         kernel,
         out_shape=jax.ShapeDtypeStruct((C, R, 256), bf16),
-        in_specs=[hbm, vmem, vmem, vmem, hbm, hbm],
+        in_specs=[hbm] * 6,
         out_specs=hbm,
         scratch_shapes=[
             pltpu.VMEM((C, 4, Q, 256), bf16),
+            pltpu.VMEM((1, 256), f32),
+            pltpu.VMEM((4, 2, 1, 512), f32),
+            pltpu.VMEM((1, 256), f32),
             pltpu.VMEM((C, 4, Q, 1024), bf16),
             pltpu.VMEM((2, 4, 2, 128, 512), bf16),
             pltpu.VMEM((4, 2, 512, 256), bf16),
@@ -379,14 +413,14 @@
             pltpu.VMEM((C, 1, R), f32),
             pltpu.VMEM((C, 15, 1, R), f32),
             pltpu.VMEM((C, R, 256), bf16),
-            dma((9,)),
-            dma((4, C)),
-            dma((4, 2 * C)),
+            dma((10,)),
+            dma((5, C)),
+            dma((2, 2 * C)),
             dma((5 + C,)),
             dma((6,)),
             dma((6, 3)),
-            dma((7,)),
-            dma((C,)),
+            dma((10,)),
+            dma((1,)),
         ],
         compiler_params=pltpu.CompilerParams(
             collective_id=0, has_side_effects=True, vmem_limit_bytes=VMEM_LIMIT

time: 105 us -> 99.8 us (0.950)
  Pallas kernels: 102 us -> 97.6 us
    pallas_call x1, Pallas kernels: 102 us -> 97.6 us  [body(): pl.pallas_call(kernel, out_shape=jax.ShapeDtypeStruct((C, R, 256), bf16),...]
where the time goes in v3:
time: 99.8 us; the launch traced here: 99.7 us
  Pallas kernels  97.6 us (98%)
  local copies, waits for them, and re-layouts  2.06 us (2%)
    pallas_call x1, Pallas kernels, body(): pl.pallas_call(kernel, out_shape=jax.ShapeDtypeStruct((C, R, 256), bf16),...  97.6 us
    unnamed x1, local copies, waits for them, and re-layouts  2.06 us

profile of v3, /device:TPU:0, one launch (start us, length us, event | category | flops | bytes accessed | tf_op | source)
XLA Modules:
  0.0 99.7 jit_solution(1380169558599531951)
XLA Ops:
  0.0 97.6 %shard_map.64 = bf16[12,128,256]{2,1,0:T(8,128)(2,1)} custom-call(bf16[12,4,32,256]{3,2,1,0:T(8,128)(2,1)} %bitcast.6, f32[1,256]{1,0:T(1,128)} %bitcast.8, f32[4,2,1,512]{3,2,1,0:T(1,128)} %bitcast.7, f32[1,256]{1,0:T(1,128)} %bitcast.9, bf16[256,4096]{1,0:T(8,128)(2,1)} %up_hbm.1, bf16[4096,256]{1,0:T(8,128)(2,1)} %down_hbm.1), custom_call_target="tpu_custom_call" | custom-call | tf_op jit(solution)/shard_map/pallas_call | solution.py:386
  97.6 2.1 %copy.8 = bf16[1536,256]{1,0:T(8,128)(2,1)} copy(bf16[1536,256]{1,0:T(8,128)(2,1)} %bitcast.5) | data formatting | bytes 1572864

commit v4 on v3

--- a/solution.py
+++ b/solution.py
@@ -32,7 +32,7 @@
 def kernel(
     tok_hbm, pre_gain_hbm, up_bias_hbm, post_gain_hbm, up_hbm, down_hbm, out_hbm,
     tok, pre_gain, up_bias, post_gain, xg, wu, wd, pf, ps, r1, rs, pr, hg, os, of, zr, xa, inv_row, inv_col, e_own, e_in, be, be_in, out,
-    ssem, csem, usem, esem, wssem, wrsem, lsem, osem,
+    ssem, csem, usem, esem, wssem, wrsem, hsem, lsem, osem,
 ):
     G = GROUP
     C, _, Q, _ = tok.shape
@@ -79,18 +79,18 @@
         "a1": (5, "y", (1, 3), lambda u, j: hg.at[u, y], lambda u, j: hg.at[u, y], lambda u: hg.at[u, 0:2]),
         "a2": (6, "y", (1, 3), lambda u, j: hg.at[u, (y + 4 - j) % 4, :, halves[side(j)]],
                lambda u, j: hg.at[u, (y + 4 - j) % 4, :, halves[side(j)]], lambda u: r1.at[u]),
-        "zr": (7, "z", (1, 3, 2), lambda c, j: os.at[c, (z + j) % 4], lambda c, j: zr.at[c, j - 1], lambda c: zr.at[c]),
-        "xa": (8, "x", (1, 3, 2), lambda c, j: xa.at[c, x], lambda c, j: xa.at[c, x], lambda c: zr.at[c]),
+        "zr": (7, "z", (2, 1, 3), lambda c, j: os.at[c, (z + j) % 4], lambda c, j: zr.at[c, j - 1], lambda c: zr.at[c]),
+        "xa": (8, "x", (2, 1, 3), lambda c, j: xa.at[c, x], lambda c, j: xa.at[c, x], lambda c: zr.at[c]),
     }
     sent = {
         "xz": xa.at[:, 0:3, 0:Q], "xx": xg.at[:, 0:2], "xf": xg.at[:, 0], "r1": r1, "rd": r1, "r2": r1, "a1": hg.at[:, 0:2],
         "a2": r1, "zr": zr, "xa": zr,
     }
-    by_chunk = {"xz": 0, "xx": 1, "zr": 2, "xa": 3, "xf": 4}
+    by_chunk = {"xz": 0, "xx": 1, "zr": 2, "xa": 0, "xf": 3}
     by_unit = {"r1": 0, "rd": 1, "r2": 1, "a1": 0, "a2": 1}
 
     def landed(name, i):
-        return csem.at[by_chunk[name], i] if name in by_chunk else usem.at[by_unit[name], i]
+        return csem.at[by_chunk[name], i] if name in by_chunk else usem.at[by_unit[name], i % 12]
 
     def send(name, i):
         n, axis, offsets, src, dst, _ = phases[name]
@@ -120,7 +120,7 @@
 
     def hand(w, n, j, half):
         at = w.at[(z + 4 - j) % 4, half]
-        return rdma(at, at, wssem.at[n + 3], wrsem.at[n + 3, j - 1], "k", 0)
+        return rdma(at, at, wssem.at[n + 3], hsem.at[n], "k", 0)
 
     def take(w, n):
         with jax.named_scope("wait_w"):
@@ -130,8 +130,8 @@
 
     def have(w, n):
         with jax.named_scope("wait_hand"):
-            for j in (1, 3, 2):
-                hand(w, n, j, 1 - k).wait_recv()
+            blocks = w.at[0:3, 0]
+            pltpu.make_async_copy(blocks, blocks, hsem.at[n]).wait()
 
     def send_energy(n):
         for j in (1, 3, 2):
@@ -144,27 +144,27 @@
 
     def send_rows(c):
         for j in range(1, 16):
-            rdma(be.at[c], be_in.at[c, j - 1], esem.at[4], esem.at[5 + c], "r", j).start()
+            rdma(be.at[c], be_in.at[c, j - 1], esem.at[4], landed("xx", c), "r", j).start()
 
     barrier = pltpu.get_barrier_semaphore()
     partners = [(axis, j) for axis in "xyz" for j in (1, 2, 3)] + [("k", 0)]
     for axis, j in partners:
         pl.semaphore_signal(barrier, inc=1, device_id=peer(axis, j), device_id_type=MESH)
 
-    load = pltpu.make_async_copy(tok_hbm, tok, lsem.at[6])
+    load = pltpu.make_async_copy(tok_hbm, tok, lsem.at[0])
     load.start()
     small = []
     for n, (far, near) in enumerate(((pre_gain_hbm, pre_gain), (up_bias_hbm, up_bias), (post_gain_hbm, post_gain))):
-        small.append(pltpu.make_async_copy(far, near, lsem.at[7 + n]))
+        small.append(pltpu.make_async_copy(far, near, lsem.at[1 + n]))
         small[-1].start()
     own = []
     for half in range(2):
         for h in range(2):
             own.append(pltpu.make_async_copy(
                 up_hbm.at[pl.ds(half * 128, 128), pl.ds(pl.multiple_of(z * 1024 + h * 512, 512), 512)],
-                wu.at[h, z, half], lsem.at[half * 2 + h]))
+                wu.at[h, z, half], lsem.at[4]))
         own.append(pltpu.make_async_copy(
-            down_hbm.at[pl.ds(pl.multiple_of(z * 1024 + half * 512, 512), 512), :], wd.at[z, half], lsem.at[4 + half]))
+            down_hbm.at[pl.ds(pl.multiple_of(z * 1024 + half * 512, 512), 512), :], wd.at[z, half], lsem.at[5]))
     for o in own:
         o.start()
     load.wait()
@@ -220,8 +220,8 @@
         spread(c)
     for c in range(AHEAD, EAGER):
         forward(c)
-    for o in own:
-        o.wait()
+    for n, blocks in ((4, wu.at[:, 0]), (5, wd.at[0])):
+        pltpu.make_async_copy(blocks, blocks, lsem.at[n]).wait()
     have(wu.at[0], 0)
 
     def energy_over_z():
@@ -309,7 +309,7 @@
     def finish(u):
         c = last_of(u)
         with jax.named_scope("wait_be"):
-            pltpu.make_async_copy(be_in.at[c], be_in.at[c], esem.at[5 + c]).wait()
+            pltpu.make_async_copy(be_in.at[c], be_in.at[c], landed("xx", c)).wait()
         total = be[c]
         for j in range(15):
             total = total + be_in[c, j]
@@ -414,12 +414,13 @@
             pltpu.VMEM((C, 15, 1, R), f32),
             pltpu.VMEM((C, R, 256), bf16),
             dma((10,)),
-            dma((5, C)),
-            dma((2, 2 * C)),
-            dma((5 + C,)),
+            dma((4, C)),
+            dma((2, 12)),
+            dma((5,)),
             dma((6,)),
-            dma((6, 3)),
-            dma((10,)),
+            dma((3, 3)),
+            dma((3,)),
+            dma((6,)),
             dma((1,)),
         ],
         compiler_params=pltpu.CompilerParams(

time: 99.8 us -> 99 us (level)
  no operation moved by 1% of the time
where the time goes in v4:
time: 99 us; the launch traced here: 98.8 us
  Pallas kernels  96.8 us (98%)
  local copies, waits for them, and re-layouts  2.06 us (2%)
    pallas_call x1, Pallas kernels, body(): pl.pallas_call(kernel, out_shape=jax.ShapeDtypeStruct((C, R, 256), bf16),...  96.8 us
    unnamed x1, local copies, waits for them, and re-layouts  2.06 us

profile of v4, /device:TPU:0, one launch (start us, length us, event | category | flops | bytes accessed | tf_op | source)
XLA Modules:
  0.0 98.8 jit_solution(18212996378911079665)
XLA Ops:
  0.0 96.8 %shard_map.64 = bf16[12,128,256]{2,1,0:T(8,128)(2,1)} custom-call(bf16[12,4,32,256]{3,2,1,0:T(8,128)(2,1)} %bitcast.6, f32[1,256]{1,0:T(1,128)} %bitcast.8, f32[4,2,1,512]{3,2,1,0:T(1,128)} %bitcast.7, f32[1,256]{1,0:T(1,128)} %bitcast.9, bf16[256,4096]{1,0:T(8,128)(2,1)} %up_hbm.1, bf16[4096,256]{1,0:T(8,128)(2,1)} %down_hbm.1), custom_call_target="tpu_custom_call" | custom-call | tf_op jit(solution)/shard_map/pallas_call | solution.py:386
  96.8 2.1 %copy.8 = bf16[1536,256]{1,0:T(8,128)(2,1)} copy(bf16[1536,256]{1,0:T(8,128)(2,1)} %bitcast.5) | data formatting | bytes 1572864

commit v5 on v4

--- a/solution.py
+++ b/solution.py
@@ -151,7 +151,7 @@
     for axis, j in partners:
         pl.semaphore_signal(barrier, inc=1, device_id=peer(axis, j), device_id_type=MESH)
 
-    load = pltpu.make_async_copy(tok_hbm, tok, lsem.at[0])
+    load = pltpu.make_async_copy(tok_hbm.at[:, x], tok.at[:, x], lsem.at[0])
     load.start()
     small = []
     for n, (far, near) in enumerate(((pre_gain_hbm, pre_gain), (up_bias_hbm, up_bias), (post_gain_hbm, post_gain))):
@@ -165,10 +165,14 @@
                 wu.at[h, z, half], lsem.at[4]))
         own.append(pltpu.make_async_copy(
             down_hbm.at[pl.ds(pl.multiple_of(z * 1024 + half * 512, 512), 512), :], wd.at[z, half], lsem.at[5]))
+    small[0].wait()
+    load.wait()
+    for j in (1, 2, 3):
+        at = (x + j) % 4
+        pltpu.make_async_copy(tok_hbm.at[:, at], tok.at[:, at], lsem.at[6]).start()
     for o in own:
         o.start()
-    load.wait()
-    for o in small:
+    for o in small[1:]:
         o.wait()
 
     gain = pre_gain[...]
@@ -193,6 +197,8 @@
     for j in (1, 3, 2):
         up_block(0, j).start()
     with jax.named_scope("own_energy"):
+        others = tok.at[:, 0:3]
+        pltpu.make_async_copy(others, others, lsem.at[6]).wait()
         lax.fori_loop(0, C, own_energy, 0)
     send_energy(0)
     for c in range(FIRST, early):
@@ -420,7 +426,7 @@
             dma((6,)),
             dma((3, 3)),
             dma((3,)),
-            dma((6,)),
+            dma((7,)),
             dma((1,)),
         ],
         compiler_params=pltpu.CompilerParams(

time: 99 us -> 99 us (level)
  no operation moved by 1% of the time
where the time goes in v5:
time: 99 us; the launch traced here: 98.8 us
  Pallas kernels  96.8 us (98%)
  local copies, waits for them, and re-layouts  2.06 us (2%)
    pallas_call x1, Pallas kernels, body(): pl.pallas_call(kernel, out_shape=jax.ShapeDtypeStruct((C, R, 256), bf16),...  96.8 us
    unnamed x1, local copies, waits for them, and re-layouts  2.06 us

profile of v5, /device:TPU:0, one launch (start us, length us, event | category | flops | bytes accessed | tf_op | source)
XLA Modules:
  0.0 98.8 jit_solution(1392209057307589906)
XLA Ops:
  0.0 96.8 %shard_map.64 = bf16[12,128,256]{2,1,0:T(8,128)(2,1)} custom-call(bf16[12,4,32,256]{3,2,1,0:T(8,128)(2,1)} %bitcast.6, f32[1,256]{1,0:T(1,128)} %bitcast.8, f32[4,2,1,512]{3,2,1,0:T(1,128)} %bitcast.7, f32[1,256]{1,0:T(1,128)} %bitcast.9, bf16[256,4096]{1,0:T(8,128)(2,1)} %up_hbm.1, bf16[4096,256]{1,0:T(8,128)(2,1)} %down_hbm.1), custom_call_target="tpu_custom_call" | custom-call | tf_op jit(solution)/shard_map/pallas_call | solution.py:392
  96.8 2.1 %copy.8 = bf16[1536,256]{1,0:T(8,128)(2,1)} copy(bf16[1536,256]{1,0:T(8,128)(2,1)} %bitcast.5) | data formatting | bytes 1572864
